TPU v7x, 32 devices: a whole 2x2x4 slice. The times are simulated.
32 devices in a mesh: sp: 8 (over z, x), tp: 4 (over y, core).
Axes of the slice: x: 2, y: 2, z: 4, core: 2. Of those that a mesh axis runs over, the one named last changes fastest.
Arguments:
- sequence_activations: bfloat16 [4096, 2048], P('sp', 'tp'), may hold values from -45 to 45
- entry_rescale_vector: float32 [2048], replicated, may hold values from 0.1 to 1.9
- blender_exit_switch_matrix: bfloat16 [2048, 2048], P('sp', 'tp'), may hold values from -0.125 to 0.125
- blender_entry_switch_matrix: bfloat16 [2048, 2048], P('sp', 'tp'), may hold values from -0.125 to 0.125
- blender_payload_matrix: bfloat16 [2048, 2048], P('sp', 'tp'), may hold values from -0.125 to 0.125
- scan_entry_matrix: bfloat16 [2048, 2048], P('sp', 'tp'), may hold values from -0.125 to 0.125
- scan_exit_switch_matrix: bfloat16 [2048, 2048], P('sp', 'tp'), may hold values from -0.125 to 0.125
- filter_blend_matrix: bfloat16 [2048, 2048], P('sp', 'tp'), may hold values from -0.125 to 0.125
- scan_blend_matrix: bfloat16 [2048, 2048], P('sp', 'tp'), may hold values from -0.125 to 0.125
- blender_kernel_coefficients: bfloat16 [3, 2048], P(None, 'tp'), may hold values from -3.5 to 3.5
- scan_kernel_coefficients: bfloat16 [4, 2048], P(None, 'tp'), may hold values from -3 to 3
- scan_switch_blockwise: bfloat16 [8, 256, 256], P('tp'), may hold values from -0.375 to 0.375
- entry_switch_blockwise: bfloat16 [8, 256, 256], P('tp'), may hold values from -0.375 to 0.375
- feature_fade_odds: float32 [2048], P('tp'), may hold values from 3 to 16
- fade_speed_multiplier: float32 [4096], P('sp'), may hold values from 0.3 to 2.8
- added_rate_shift: float32 [4096], P('sp'), may hold values from -1.4 to 0
- initial_hidden_vector: float32 [2048], P('tp'), may hold values from -6 to 6
- filter_exit_matrix: bfloat16 [2048, 2048], P('tp'), may hold values from -0.125 to 0.125
- scan_exit_matrix: bfloat16 [2048, 2048], P('tp'), may hold values from -0.125 to 0.125
Outputs:
- mixed: bfloat16 [4096, 2048], P('sp', 'tp')
All inputs are finite; a program needn't handle non-finite values.
Results may differ from a plain program's by a relative error of at most 0.015.
Values may be sent and summed in bfloat16 or wider, within the bound.
A program may use at most 64 MiB of HBM per device.

v0:
```python
import jax
import jax.numpy as jnp
from jax import lax
from jax.sharding import PartitionSpec as P

scan_switch_exponent = 8.0
norm_eps = 1e-06


def passed_along(value, axis, by):
    peers = lax.axis_size(axis)
    pairs = [(i, i + by) for i in range(peers) if 0 <= i + by < peers]
    return lax.ppermute(value, axis, pairs)


def entering(value, axis, combine, identity):
    peers, place = (lax.axis_size(axis), lax.axis_index(axis))
    everything = jax.tree.map(lambda part: lax.all_gather(part, axis), value)
    start = jax.tree.map(
        lambda part, zero: jnp.broadcast_to(jnp.asarray(zero, part.dtype), part.shape),
        value,
        identity,
    )

    def step(k, before):
        reached = k < place
        new = combine(before, jax.tree.map(lambda part: part[k], everything))
        return jax.tree.map(lambda a, b: jnp.where(reached, a, b), new, before)

    return lax.fori_loop(0, peers, step, start)


def linear_chain(earlier, later):
    return (earlier[0] * later[0], later[0] * earlier[1] + later[1])


def causal_local(previous, values, weights):
    taps = weights.shape[0]
    length = values.shape[0]
    extended = jnp.concatenate([previous, values], axis=0)
    result = extended[0:length] * weights[0].astype(jnp.float32)
    for tap_index in range(1, taps):
        result = result + extended[tap_index : tap_index + length] * weights[tap_index].astype(
            jnp.float32
        )
    return result


def local(
    sequence_activations,
    entry_rescale_vector,
    blender_exit_switch_matrix,
    blender_entry_switch_matrix,
    blender_payload_matrix,
    scan_entry_matrix,
    scan_exit_switch_matrix,
    filter_blend_matrix,
    scan_blend_matrix,
    blender_kernel_coefficients,
    scan_kernel_coefficients,
    scan_switch_blockwise,
    entry_switch_blockwise,
    feature_fade_odds,
    fade_speed_multiplier,
    added_rate_shift,
    initial_hidden_vector,
    filter_exit_matrix,
    scan_exit_matrix,
):
    row_count = sequence_activations.shape[0]
    feature_count = entry_rescale_vector.shape[0]
    pieces = [
        blender_exit_switch_matrix,
        blender_entry_switch_matrix,
        blender_payload_matrix,
        scan_entry_matrix,
        scan_exit_switch_matrix,
        filter_blend_matrix,
        scan_blend_matrix,
    ]
    local_cat = jnp.concatenate(pieces, axis=1)
    whole_weight = lax.all_gather(local_cat, "sp", axis=0, tiled=True)
    piece = lax.all_gather(sequence_activations, "tp", axis=1, tiled=True)
    piece_float = piece.astype(jnp.float32)
    scaled_piece = (piece.astype(jnp.float32) * entry_rescale_vector[None, :]).astype(jnp.bfloat16)
    totals = jnp.dot(scaled_piece, whole_weight, preferred_element_type=jnp.float32)
    squares = jnp.sum(piece_float * piece_float, axis=1)
    inverse = lax.rsqrt(squares / feature_count + norm_eps)
    projected = (totals * inverse[:, None]).astype(jnp.bfloat16)
    outputs = []
    offset = 0
    for weight in pieces:
        outputs.append(projected[:, offset : offset + weight.shape[1]])
        offset = offset + weight.shape[1]
    conv_b, conv_c, conv_x, lru_in, lru_gate, mix_conv, mix_lru = outputs
    short_in = conv_c.astype(jnp.float32) * conv_x.astype(jnp.float32)
    lru_float = lru_in.astype(jnp.float32)
    short_edge = blender_kernel_coefficients.shape[0] - 1
    lru_edge = scan_kernel_coefficients.shape[0] - 1
    prev_short, prev_lru = passed_along(
        (short_in[row_count - short_edge :], lru_float[row_count - lru_edge :]), "sp", 1
    )
    lru_conv = causal_local(prev_lru, lru_float, scan_kernel_coefficients).astype(jnp.bfloat16)
    head_local = scan_switch_blockwise.shape[0]
    head_size = scan_switch_blockwise.shape[1]
    lru_local = lru_conv.shape[1]
    heads = lru_conv.reshape(row_count, head_local, head_size)
    scan_switch_amount = jax.nn.sigmoid(
        jnp.einsum("thi,hij->thj", heads, scan_switch_blockwise, preferred_element_type=jnp.float32)
    ).reshape(row_count, lru_local)
    gate_i = jax.nn.sigmoid(
        jnp.einsum(
            "thi,hij->thj", heads, entry_switch_blockwise, preferred_element_type=jnp.float32
        )
    ).reshape(row_count, lru_local)
    position = lax.axis_index("sp") * row_count + jnp.arange(row_count, dtype=jnp.int32)
    fade_exponent_multiplier = (
        scan_switch_exponent
        * scan_switch_amount
        * jax.nn.log_sigmoid(feature_fade_odds)[None, :]
        * fade_speed_multiplier[:, None]
        + added_rate_shift[:, None]
    )
    decay = jnp.exp(fade_exponent_multiplier)
    scale = jnp.sqrt(-jnp.expm1(2.0 * fade_exponent_multiplier))
    scale = jnp.where((position == 0)[:, None], jnp.float32(1.0), scale)
    drive = scale * gate_i * lru_conv.astype(jnp.float32)
    cum_decay, cum_drive = lax.associative_scan(linear_chain, (decay, drive), axis=0)
    ones_state = jnp.ones((lru_local,), jnp.float32)
    zero_state = jnp.zeros((lru_local,), jnp.float32)
    pref_decay, pref_state = entering(
        (cum_decay[-1], cum_drive[-1]), "sp", linear_chain, (ones_state, zero_state)
    )
    carry_in = pref_decay * initial_hidden_vector + pref_state
    state = cum_drive + cum_decay * carry_in[None, :]
    lru_mix = (state * jax.nn.gelu(lru_gate.astype(jnp.float32), approximate=True)).astype(
        jnp.bfloat16
    )
    conv_mix = (
        conv_b.astype(jnp.float32) * causal_local(prev_short, short_in, blender_kernel_coefficients)
    ).astype(jnp.bfloat16)
    conv_part = jnp.dot(conv_mix, filter_exit_matrix, preferred_element_type=jnp.float32)
    lru_part = jnp.dot(lru_mix, scan_exit_matrix, preferred_element_type=jnp.float32)
    conv_sum, lru_sum = (
        lax.psum_scatter(
            conv_part.astype(jnp.bfloat16), "tp", scatter_dimension=1, tiled=True
        ).astype(jnp.float32),
        lax.psum_scatter(
            lru_part.astype(jnp.bfloat16), "tp", scatter_dimension=1, tiled=True
        ).astype(jnp.float32),
    )
    mixed = (
        jax.nn.sigmoid(mix_conv.astype(jnp.float32)) * conv_sum
        + jax.nn.sigmoid(mix_lru.astype(jnp.float32)) * lru_sum
    )
    return mixed.astype(jnp.bfloat16)


def solution(mesh):
    placed = (
        P("sp", "tp"),
        P(),
        P("sp", "tp"),
        P("sp", "tp"),
        P("sp", "tp"),
        P("sp", "tp"),
        P("sp", "tp"),
        P("sp", "tp"),
        P("sp", "tp"),
        P(None, "tp"),
        P(None, "tp"),
        P("tp", None, None),
        P("tp", None, None),
        P("tp"),
        P("sp"),
        P("sp"),
        P("tp"),
        P("tp", None),
        P("tp", None),
    )
    return jax.shard_map(
        local, mesh=mesh, in_specs=placed, out_specs=P("sp", "tp"), check_vma=False
    )
```

profile of v0, /device:TPU:0, one launch (start us, length us, event | category | flops | bytes accessed | tf_op | source)
XLA Modules:
  0.0 475.5 jit_solution(15577859545988110399)
XLA Ops:
  7.3 1.7 constant_dynamic-update-slice_fusion.6
  9.0 1.7 constant_dynamic-update-slice_fusion.5
  10.7 1.7 constant_dynamic-update-slice_fusion.4
  15.7 18.6 %all-gather.5.cloned.1.call-done = bf16[512,2048]{1,0:T(8,128)(2,1)} async-done(((bf16[512,512]{1,0:T(8,128)(2,1)}), bf16[512,2048]{1,0:T(8,128)(2,1)}) %all-gather.5.cloned.1.call-update) | async-done | bytes 2097168 | tf_op jit(solution)/shard_map/all_gather | solution.py:83
  34.2 2.1 fusion.1
  36.3 201.8 %all-gather.7.cloned.1.call-done = bf16[2048,3584]{1,0:T(8,128)(2,1)} async-done(((bf16[256,3584]{1,0:T(8,128)(2,1)}), bf16[2048,3584]{1,0:T(8,128)(2,1)}) %all-gather.7.cloned.1.call-update) | async-done | bytes 14680080 | tf_op jit(solution)/shard_map/all_gather | solution.py:82
  238.1 11.6 %multiply_convert_fusion = bf16[512,3584]{1,0:T(8,128)(2,1)S(1)} fusion(bf16[2048,3584]{1,0:T(8,128)(2,1)} %all-gather.7.cloned.1.call-done, f32[512]{0:T(512)S(1)} %add_rsqrt_fusion, bf16[512,2048]{1,0:T(8,128)(2,1)} %all-gather.5.cloned.1.call-done, f32[2048]{0:T(1024)S(1)} %copy-done.51), kind=kOutput, calls=%fused_computation.4 | convolution fusion | flops 7523008512 | bytes 20457472 | tf_op jit(solution)/shard_map/dot_general | solution.py:86
  250.0 2.5 collective-permute-start
  252.6 2.5 collective-permute-start.1
  255.1 2.8 convolution_convert_fusion.1
  260.8 1.3 copy.35
  262.1 2.6 convert_multiply_fusion.5
  264.7 2.1 slice.352
  266.8 2.1 slice.353
  268.9 2.1 slice.351
  271.0 2.1 slice.355
  273.0 2.0 multiply_add_fusion.1
  275.0 1.4 slice.358
  276.4 1.4 slice.359
  277.8 1.4 slice.357
  279.1 1.4 slice.361
  280.5 2.0 multiply_add_fusion.2
  283.9 1.6 slice.363
  285.5 1.6 slice.367
  287.1 1.8 multiply_add_fusion.3
  290.2 1.5 slice.369
  291.7 1.5 slice.373
  293.2 1.6 multiply_add_fusion.4
  294.9 1.5 slice.376
  296.3 1.4 slice.377
  297.8 1.5 slice.375
  299.2 1.5 slice.379
  300.7 1.4 multiply_add_fusion.5
  302.1 1.4 slice.382
  303.5 1.4 slice.383
  304.8 1.4 slice.381
  306.2 1.4 slice.385
  307.5 1.4 multiply_add_fusion.6
  310.1 1.3 slice.387
  311.4 1.3 slice.391
  312.8 1.4 multiply_add_fusion.7
  320.1 1.4 fusion.68
  322.1 1.3 slice.386
  326.7 1.4 slice.405
  330.6 1.5 slice.374
  332.1 1.5 slice.407
  336.2 1.5 slice.368
  344.1 1.4 slice.356
  345.5 1.4 slice.413
  348.1 2.1 slice.350
  350.2 2.1 slice.415
  354.7 1.9 fusion.51
  357.8 1.7 pad_maximum_fusion.5
  359.5 2.6 pad.142
  362.1 1.7 pad.143
  363.8 2.9 fusion.39
  367.7 4.6 pad.127
  373.3 26.1 %all-gather.1 = f32[8,1,512]{2,1,0:T(1,128)S(1)} all-gather(f32[1,1,512]{2,1,0:T(1,128)S(1)} %add_bitcast_fusion), channel_id=1, replica_groups=mesh['sp'=8,'tp'=4] {'sp'}, dimensions={0}, use_global_device_ids=true | all-gather | bytes 18432 | tf_op jit(solution)/shard_map/all_gather | solution.py:18
  399.5 2.7 pad.145
  402.3 2.7 pad.144
  405.7 26.1 %all-gather = f32[8,1,512]{2,1,0:T(1,128)S(1)} all-gather(f32[1,1,512]{2,1,0:T(1,128)S(1)} %add_bitcast_fusion.1), channel_id=1, replica_groups=mesh['sp'=8,'tp'=4] {'sp'}, dimensions={0}, use_global_device_ids=true | all-gather | bytes 18432 | tf_op jit(solution)/shard_map/all_gather | solution.py:18
  432.3 5.3 %convolution_convert_fusion = bf16[512,2048]{1,0:T(8,128)(2,1)} fusion(bf16[512,2048]{1,0:T(8,128)(2,1)} %param.39, f32[512,512]{1,0:T(8,128)} %pad.144, f32[512,512]{1,0:T(8,128)} %pad.145, f32[512,512]{1,0:T(8,128)S(1)} %copy-done.10, f32[512,512]{1,0:T(8,128)S(1)} %copy-done.8, bf16[512,3584]{1,0:T(8,128)(2,1)} %copy-done.7, f32[512]{0:T(512)S(1)} %multiply_add_fusion.9), kind=kOutput, calls=%fused_computation.9 | convolution fusion | flops 1078722560 | bytes 8914944 | tf_op jit(solution)/shard_map/dot_general | solution.py:143
  437.7 28.3 %reduce-scatter.5.cloned.1.call-done = bf16[512,512]{1,0:T(8,128)(2,1)} async-done(((bf16[512,2048]{1,0:T(8,128)(2,1)}), bf16[512,512]{1,0:T(8,128)(2,1)}) %reduce-scatter.5.cloned.1.call-update) | async-done | bytes 524304 | tf_op jit(solution)/shard_map/reduce_scatter | solution.py:148
  466.1 2.9 add_convert_fusion
  (248 shorter events, 39.9 us)
Async XLA Ops:
  6.5 248.5 %copy-start = (bf16[512,2048]{1,0:T(8,128)(2,1)S(1)}, bf16[512,2048]{1,0:T(8,128)(2,1)}, u32[]{:S(2)}) copy-start(bf16[512,2048]{1,0:T(8,128)(2,1)} %param.38) | copy-start | bytes 6291460
  6.5 5.9 %copy-start.12 = (bf16[256,512]{1,0:T(8,128)(2,1)S(1)}, bf16[256,512]{1,0:T(8,128)(2,1)}, u32[]{:S(2)}) copy-start(bf16[256,512]{1,0:T(8,128)(2,1)} %param.26) | copy-start | bytes 786436
  6.5 6.6 %copy-start.13 = (bf16[256,512]{1,0:T(8,128)(2,1)S(1)}, bf16[256,512]{1,0:T(8,128)(2,1)}, u32[]{:S(2)}) copy-start(bf16[256,512]{1,0:T(8,128)(2,1)} %param.27) | copy-start | bytes 786436
  6.5 7.4 %copy-start.14 = (bf16[256,512]{1,0:T(8,128)(2,1)S(1)}, bf16[256,512]{1,0:T(8,128)(2,1)}, u32[]{:S(2)}) copy-start(bf16[256,512]{1,0:T(8,128)(2,1)} %param.28) | copy-start | bytes 786436
  6.5 8.1 %copy-start.15 = (bf16[256,512]{1,0:T(8,128)(2,1)S(1)}, bf16[256,512]{1,0:T(8,128)(2,1)}, u32[]{:S(2)}) copy-start(bf16[256,512]{1,0:T(8,128)(2,1)} %param.29) | copy-start | bytes 786436
  6.5 27.7 %all-gather.5.cloned.1.call-start = ((), (), s32[]{:S(2)}) async-start(), calls=%async_computation.2 | async-start | bytes 2621440 | tf_op jit(solution)/shard_map/all_gather | solution.py:83
  7.3 230.9 %all-gather.7.cloned.1.call-start = ((), (), s32[]{:S(2)}) async-start(), calls=%async_computation.3 | async-start | bytes 16515072 | tf_op jit(solution)/shard_map/all_gather | solution.py:82
  12.4 3.2 copy-start.47
  12.4 3.2 copy-start.28
  12.4 3.2 copy-start.25
  15.5 222.7 %copy-start.51 = (f32[2048]{0:T(1024)S(1)}, f32[2048]{0:T(1024)}, u32[]{:S(2)}) copy-start(f32[2048]{0:T(1024)} %param.22) | copy-start | bytes 24580
  15.5 422.3 %reduce-scatter.3.cloned.1.call-start = ((), (), s32[]{:S(2)}) async-start(), calls=%async_computation.4 | async-start | bytes 2621440 | tf_op jit(solution)/shard_map/reduce_scatter | solution.py:145
  249.8 5.3 %copy-start.7 = (bf16[512,3584]{1,0:T(8,128)(2,1)}, bf16[512,3584]{1,0:T(8,128)(2,1)S(1)}, u32[]{:S(2)}) copy-start(bf16[512,3584]{1,0:T(8,128)(2,1)S(1)} %multiply_convert_fusion) | copy-start | bytes 11010052
  250.0 5.1 %collective-permute-start = (f32[2,512]{1,0:T(2,128)S(1)}, f32[2,512]{1,0:T(2,128)S(1)}, u32[]{:S(2)}, u32[]{:S(2)}) collective-permute-start(f32[2,512]{1,0:T(2,128)S(1)} %slice.440), channel_id=1, source_target_pairs={{0,4},{4,8},{8,12},{12,16},{16,20},{20,24},{24,28},{1,5},{5,9},{9,... | collective-permute-start | bytes 12296 | tf_op jit(solution)/shard_map/ppermute | solution.py:13
  252.6 5.5 %collective-permute-start.1 = (f32[3,512]{1,0:T(4,128)S(1)}, f32[3,512]{1,0:T(4,128)S(1)}, u32[]{:S(2)}, u32[]{:S(2)}) collective-permute-start(f32[3,512]{1,0:T(4,128)S(1)} %slice.445), channel_id=1, source_target_pairs={{0,4},{4,8},{8,12},{12,16},{16,20},{20,24},{24,28},{1,5},{5,9},{9,... | collective-permute-start | bytes 18440 | tf_op jit(solution)/shard_map/ppermute | solution.py:13
  257.9 0.9 copy-start.49
  257.9 208.2 %reduce-scatter.5.cloned.1.call-start = ((), (), s32[]{:S(2)}) async-start(), calls=%async_computation.5 | async-start | bytes 2621440 | tf_op jit(solution)/shard_map/reduce_scatter | solution.py:148
  258.6 1.1 copy-start.4
  259.3 1.0 copy-start.50
  260.7 1.3 copy-start.45
  260.8 1.3 copy-start.46
  343.9 8.4 %copy-start.41 = (f32[1,512]{1,0:T(1,128)S(1)}, f32[1,512]{1,0:T(1,128)}, u32[]{:S(2)}) copy-start(f32[1,512]{1,0:T(1,128)} %get-tuple-element.182) | copy-start | bytes 6148
  343.9 8.4 %copy-start.42 = (f32[1,512]{1,0:T(1,128)S(1)}, f32[1,512]{1,0:T(1,128)}, u32[]{:S(2)}) copy-start(f32[1,512]{1,0:T(1,128)} %get-tuple-element.183) | copy-start | bytes 6148
  343.9 8.4 %copy-start.43 = (f32[1,512]{1,0:T(1,128)S(1)}, f32[1,512]{1,0:T(1,128)}, u32[]{:S(2)}) copy-start(f32[1,512]{1,0:T(1,128)} %get-tuple-element.184) | copy-start | bytes 6148
  343.9 8.4 %copy-start.44 = (f32[1,512]{1,0:T(1,128)S(1)}, f32[1,512]{1,0:T(1,128)}, u32[]{:S(2)}) copy-start(f32[1,512]{1,0:T(1,128)} %get-tuple-element.185) | copy-start | bytes 6148
  343.9 8.4 %copy-start.27 = (f32[2,512]{1,0:T(2,128)S(1)}, f32[2,512]{1,0:T(2,128)}, u32[]{:S(2)}) copy-start(f32[2,512]{1,0:T(2,128)} %get-tuple-element.202) | copy-start | bytes 12292
  344.0 8.4 %copy-start.26 = (f32[2,512]{1,0:T(2,128)S(1)}, f32[2,512]{1,0:T(2,128)}, u32[]{:S(2)}) copy-start(f32[2,512]{1,0:T(2,128)} %get-tuple-element.201) | copy-start | bytes 12292
  344.0 8.5 %copy-start.23 = (f32[3,512]{1,0:T(4,128)S(1)}, f32[3,512]{1,0:T(4,128)}, u32[]{:S(2)}) copy-start(f32[3,512]{1,0:T(4,128)} %slice.386) | copy-start | bytes 18436
  344.0 8.5 %copy-start.24 = (f32[3,512]{1,0:T(4,128)S(1)}, f32[3,512]{1,0:T(4,128)}, u32[]{:S(2)}) copy-start(f32[3,512]{1,0:T(4,128)} %slice.403) | copy-start | bytes 18436
  344.0 8.5 %copy-start.40 = (f32[1,512]{1,0:T(1,128)S(1)}, f32[1,512]{1,0:T(1,128)}, u32[]{:S(2)}) copy-start(f32[1,512]{1,0:T(1,128)} %slice.485) | copy-start | bytes 6148
  344.0 8.6 %copy-start.39 = (f32[1,512]{1,0:T(1,128)S(1)}, f32[1,512]{1,0:T(1,128)}, u32[]{:S(2)}) copy-start(f32[1,512]{1,0:T(1,128)} %slice.456) | copy-start | bytes 6148
  344.0 8.6 %copy-start.22 = (f32[7,512]{1,0:T(8,128)S(1)}, f32[7,512]{1,0:T(8,128)}, u32[]{:S(2)}) copy-start(f32[7,512]{1,0:T(8,128)} %slice.405) | copy-start | bytes 43012
  344.0 8.7 %copy-start.38 = (f32[1,512]{1,0:T(1,128)S(1)}, f32[1,512]{1,0:T(1,128)}, u32[]{:S(2)}) copy-start(f32[1,512]{1,0:T(1,128)} %slice.484) | copy-start | bytes 6148
  344.0 8.7 %copy-start.37 = (f32[1,512]{1,0:T(1,128)S(1)}, f32[1,512]{1,0:T(1,128)}, u32[]{:S(2)}) copy-start(f32[1,512]{1,0:T(1,128)} %slice.455) | copy-start | bytes 6148
  344.0 8.8 %copy-start.18 = (f32[15,512]{1,0:T(8,128)S(1)}, f32[15,512]{1,0:T(8,128)}, u32[]{:S(2)}) copy-start(f32[15,512]{1,0:T(8,128)} %slice.374) | copy-start | bytes 92164
  344.0 8.8 %copy-start.19 = (f32[15,512]{1,0:T(8,128)S(1)}, f32[15,512]{1,0:T(8,128)}, u32[]{:S(2)}) copy-start(f32[15,512]{1,0:T(8,128)} %slice.407) | copy-start | bytes 92164
  344.1 8.8 %copy-start.36 = (f32[1,512]{1,0:T(1,128)S(1)}, f32[1,512]{1,0:T(1,128)}, u32[]{:S(2)}) copy-start(f32[1,512]{1,0:T(1,128)} %slice.483) | copy-start | bytes 6148
  345.5 7.5 %copy-start.35 = (f32[1,512]{1,0:T(1,128)S(1)}, f32[1,512]{1,0:T(1,128)}, u32[]{:S(2)}) copy-start(f32[1,512]{1,0:T(1,128)} %slice.454) | copy-start | bytes 6148
  348.1 5.0 %copy-start.16 = (f32[31,512]{1,0:T(8,128)S(1)}, f32[31,512]{1,0:T(8,128)}, u32[]{:S(2)}) copy-start(f32[31,512]{1,0:T(8,128)} %slice.368) | copy-start | bytes 190468
  348.1 5.0 %copy-start.17 = (f32[31,512]{1,0:T(8,128)S(1)}, f32[31,512]{1,0:T(8,128)}, u32[]{:S(2)}) copy-start(f32[31,512]{1,0:T(8,128)} %slice.409) | copy-start | bytes 190468
  350.2 2.9 copy-start.34
  350.2 3.0 copy-start.33
  352.6 0.9 copy-start.11
  352.9 0.7 copy-start.32
  353.1 0.7 copy-start.31
  353.8 2.8 copy-start.30
  354.7 3.1 copy-start.29
  363.7 3.9 copy-start.2
  363.7 3.9 copy-start.3
  367.6 4.7 copy-start.6
  372.4 29.8 %copy-start.5 = (f32[255,512]{1,0:T(8,128)S(1)}, f32[255,512]{1,0:T(8,128)}, u32[]{:S(2)}) copy-start(f32[255,512]{1,0:T(8,128)} %get-tuple-element.157) | copy-start | bytes 1566724
  372.6 26.9 %copy-start.9 = (f32[512,512]{1,0:T(8,128)}, f32[512,512]{1,0:T(8,128)S(1)}, u32[]{:S(2)}) copy-start(f32[512,512]{1,0:T(8,128)S(1)} %pad.126) | copy-start | bytes 3145732
  399.4 32.4 %copy-start.20 = (f32[512]{0:T(512)S(1)}, f32[512]{0:T(512)}, u32[]{:S(2)}) copy-start(f32[512]{0:T(512)} %custom-call) | copy-start | bytes 6148
  399.4 32.4 %copy-start.21 = (f32[512]{0:T(512)S(1)}, f32[512]{0:T(512)}, u32[]{:S(2)}) copy-start(f32[512]{0:T(512)} %custom-call.1) | copy-start | bytes 6148
  399.5 32.9 %copy-start.48 = (f32[512]{0:T(512)S(1)}, f32[512]{0:T(512)}, u32[]{:S(2)}) copy-start(f32[512]{0:T(512)} %param.37) | copy-start | bytes 6148
  399.5 32.9 %copy-start.8 = (f32[512,512]{1,0:T(8,128)S(1)}, f32[512,512]{1,0:T(8,128)}, u32[]{:S(2)}) copy-start(f32[512,512]{1,0:T(8,128)} %pad.127) | copy-start | bytes 3145732
  402.2 30.1 %copy-start.10 = (f32[512,512]{1,0:T(8,128)S(1)}, f32[512,512]{1,0:T(8,128)}, u32[]{:S(2)}) copy-start(f32[512,512]{1,0:T(8,128)} %copy-done.9) | copy-start | bytes 3145732
  437.7 31.3 %copy-start.1 = (bf16[512,2048]{1,0:T(8,128)(2,1)S(1)}, bf16[512,2048]{1,0:T(8,128)(2,1)}, u32[]{:S(2)}) copy-start(bf16[512,2048]{1,0:T(8,128)(2,1)} %param.38) | copy-start | bytes 6291460
Sparse Core Ops, SparseCore 0:
  8.9 25.2 all-gather.4
  36.4 201.6 all-gather.6
  258.0 30.6 reduce-scatter.2
  437.8 28.1 reduce-scatter.4
where the time goes:
time: 478 us; the launch traced here: 476 us
  waiting for transfers between devices  249 us (52%)
  local copies, waits for them, and re-layouts  100 us (21%)
  blocking collectives  52.2 us (11%)
  other arithmetic  33 us (7%)
  matrix products  20.7 us (4%)
  between operations  14.2 us (3%)
  starting transfers between devices  5.26 us (1%)
    all_gather x1, waiting for transfers between devices, local(): whole_weight = lax.all_gather(local_cat, 'sp', axis=0, tiled=True)  202 us
    slice x60, local copies, waits for them, and re-layouts, local(): lax.associative_scan(linear_chain, (decay, drive), axis=0)  73.1 us
    all_gather x2, blocking collectives, entering(): everything = jax.tree.map(lambda part: lax.all_gather(part, axis), value)  52.2 us
    reduce_scatter x1, waiting for transfers between devices, local(): lax.psum_scatter(lru_part.astype(jnp.bfloat16), 'tp', scatter_dimension=1...  28.3 us
    all_gather x1, waiting for transfers between devices, local(): piece = lax.all_gather(sequence_activations, 'tp', axis=1, tiled=True)  18.6 us
    add x16, other arithmetic, linear_chain(): return (earlier[0] * later[0], later[0] * earlier[1] + later[1])  17.2 us
    pad x32, local copies, waits for them, and re-layouts, local(): lax.associative_scan(linear_chain, (decay, drive), axis=0)  16 us
    dot_general x1, matrix products, local(): jnp.dot(scaled_piece, whole_weight, preferred_element_type=jnp.float32)  11.6 us
  transfers between devices with their start and end apart: 6, of which 3 were waited for; matrix products, arithmetic and copies ran while one was open for 29% of the time, Pallas kernels for 0%

commit v1 on v0

--- a/solution.py
+++ b/solution.py
@@ -79,7 +79,12 @@
         scan_blend_matrix,
     ]
     local_cat = jnp.concatenate(pieces, axis=1)
-    whole_weight = lax.all_gather(local_cat, "sp", axis=0, tiled=True)
+    ring = [local_cat]
+    for hop in range(7):
+        ring.append(lax.ppermute(ring[-1], "sp", [(dev, (dev + 1) % 8) for dev in range(8)]))
+    whole_weight = jnp.roll(
+        jnp.concatenate(ring[::-1], axis=0), (lax.axis_index("sp") + 1) * ring[0].shape[0], axis=0
+    )
     piece = lax.all_gather(sequence_activations, "tp", axis=1, tiled=True)
     piece_float = piece.astype(jnp.float32)
     scaled_piece = (piece.astype(jnp.float32) * entry_rescale_vector[None, :]).astype(jnp.bfloat16)

time: 478 us -> 658 us (1.38)
  local copies, waits for them, and re-layouts: 100 us -> 181 us
  waiting for transfers between devices: 249 us -> 317 us
  other arithmetic: 33 us -> 60.9 us
    ppermute x0 -> x7, waiting for transfers between devices: none -> 289 us  [local(): lax.ppermute(ring[-1], 'sp', [(dev, (dev + 1) % 8) for dev in range(8)])]
    all_gather x1 -> x0, waiting for transfers between devices: 202 us -> none  [local(): whole_weight = lax.all_gather(local_cat, 'sp', axis=0, tiled=True)]
    unnamed x112 -> x83, local copies, waits for them, and re-layouts: 8.6 us -> 55.8 us
    all_gather x1, waiting for transfers between devices: 18.6 us -> 0.02 us  [local(): piece = lax.all_gather(sequence_activations, 'tp', axis=1, tiled=True)]
    pad x32, local copies, waits for them, and re-layouts: 16 us -> 33.4 us  [local(): lax.associative_scan(linear_chain, (decay, drive), axis=0)]
    slice x60, local copies, waits for them, and re-layouts: 73.1 us -> 86.8 us  [local(): lax.associative_scan(linear_chain, (decay, drive), axis=0)]
    concatenate x15, other arithmetic: 1.95 us -> 11.3 us  [local(): lax.associative_scan(linear_chain, (decay, drive), axis=0)]
    add x15, other arithmetic: 2.5 us -> 10.4 us  [local(): lax.associative_scan(linear_chain, (decay, drive), axis=0)]
  transfers between devices with their start and end apart: 6 -> 12, of which waited for: 3 -> 8; matrix products, arithmetic and copies ran while one was open for 29% -> 29% of each run, Pallas kernels for 0% -> 0%
where the time goes in v1:
time: 658 us; the launch traced here: 653 us
  waiting for transfers between devices  317 us (48%)
  local copies, waits for them, and re-layouts  181 us (28%)
  other arithmetic  60.9 us (9%)
  blocking collectives  52.2 us (8%)
  matrix products  22.9 us (3%)
  between operations  13.6 us (2%)
    ppermute x7, waiting for transfers between devices, local(): lax.ppermute(ring[-1], 'sp', [(dev, (dev + 1) % 8) for dev in range(8)])  289 us
    slice x60, local copies, waits for them, and re-layouts, local(): lax.associative_scan(linear_chain, (decay, drive), axis=0)  86.8 us
    unnamed x83, local copies, waits for them, and re-layouts  55.8 us
    all_gather x2, blocking collectives, entering(): everything = jax.tree.map(lambda part: lax.all_gather(part, axis), value)  52.2 us
    pad x32, local copies, waits for them, and re-layouts, local(): lax.associative_scan(linear_chain, (decay, drive), axis=0)  33.4 us
    reduce_scatter x1, waiting for transfers between devices, local(): lax.psum_scatter(lru_part.astype(jnp.bfloat16), 'tp', scatter_dimension=1...  27.6 us
    add x16, other arithmetic, linear_chain(): return (earlier[0] * later[0], later[0] * earlier[1] + later[1])  23.6 us
  transfers between devices with their start and end apart: 12, of which 8 were waited for; matrix products, arithmetic and copies ran while one was open for 29% of the time, Pallas kernels for 0%

profile of v1, /device:TPU:0, one launch (start us, length us, event | category | flops | bytes accessed | tf_op | source)
XLA Modules:
  0.0 653.4 jit_solution(411651596755064644)
XLA Ops:
  13.6 3.0 collective-permute-start
  16.6 43.0 %collective-permute-done = bf16[256,3584]{1,0:T(8,128)(2,1)S(1)} collective-permute-done((bf16[256,3584]{1,0:T(8,128)(2,1)S(1)}, bf16[256,3584]{1,0:T(8,128)(2,1)S(1)}, u32[]{:S(2)}, u32[]{:S(2)}) %collective-permute-start) | collective-permute-done | bytes 1835040 | tf_op jit(solution)/shard_map/ppermute | solution.py:84
  60.9 43.9 %collective-permute-done.1 = bf16[256,3584]{1,0:T(8,128)(2,1)S(1)} collective-permute-done((bf16[256,3584]{1,0:T(8,128)(2,1)S(1)}, bf16[256,3584]{1,0:T(8,128)(2,1)S(1)}, u32[]{:S(2)}, u32[]{:S(2)}) %collective-permute-start.1) | collective-permute-done | bytes 1835040 | tf_op jit(solution)/shard_map/ppermute | solution.py:84
  106.0 43.0 %collective-permute-done.2 = bf16[256,3584]{1,0:T(8,128)(2,1)S(1)} collective-permute-done((bf16[256,3584]{1,0:T(8,128)(2,1)S(1)}, bf16[256,3584]{1,0:T(8,128)(2,1)S(1)}, u32[]{:S(2)}, u32[]{:S(2)}) %collective-permute-start.2) | collective-permute-done | bytes 1835040 | tf_op jit(solution)/shard_map/ppermute | solution.py:84
  150.3 42.2 %collective-permute-done.3 = bf16[256,3584]{1,0:T(8,128)(2,1)S(1)} collective-permute-done((bf16[256,3584]{1,0:T(8,128)(2,1)S(1)}, bf16[256,3584]{1,0:T(8,128)(2,1)S(1)}, u32[]{:S(2)}, u32[]{:S(2)}) %collective-permute-start.3) | collective-permute-done | bytes 1835040 | tf_op jit(solution)/shard_map/ppermute | solution.py:84
  193.7 41.4 %collective-permute-done.4 = bf16[256,3584]{1,0:T(8,128)(2,1)} collective-permute-done((bf16[256,3584]{1,0:T(8,128)(2,1)S(1)}, bf16[256,3584]{1,0:T(8,128)(2,1)}, u32[]{:S(2)}, u32[]{:S(2)}) %collective-permute-start.4) | collective-permute-done | bytes 1835040 | tf_op jit(solution)/shard_map/ppermute | solution.py:84
  235.2 40.7 %collective-permute-done.5 = bf16[256,3584]{1,0:T(8,128)(2,1)} collective-permute-done((bf16[256,3584]{1,0:T(8,128)(2,1)}, bf16[256,3584]{1,0:T(8,128)(2,1)}, u32[]{:S(2)}, u32[]{:S(2)}) %collective-permute-start.5) | collective-permute-done | bytes 1835040 | tf_op jit(solution)/shard_map/ppermute | solution.py:84
  278.3 2.2 fusion.5
  280.6 35.2 %collective-permute-done.6 = bf16[256,3584]{1,0:T(8,128)(2,1)} collective-permute-done((bf16[256,3584]{1,0:T(8,128)(2,1)}, bf16[256,3584]{1,0:T(8,128)(2,1)}, u32[]{:S(2)}, u32[]{:S(2)}) %collective-permute-start.6) | collective-permute-done | bytes 1835040 | tf_op jit(solution)/shard_map/ppermute | solution.py:84
  315.8 2.9 constant_dynamic-update-slice_fusion.22
  318.7 2.8 constant_dynamic-update-slice_fusion.21
  321.5 2.9 constant_dynamic-update-slice_fusion.20
  324.4 2.9 constant_dynamic-update-slice_fusion.19
  327.3 2.9 constant_dynamic-update-slice_fusion.18
  330.2 2.9 constant_dynamic-update-slice_fusion.17
  333.0 2.9 constant_dynamic-update-slice_fusion.16
  341.2 2.8 constant_dynamic-update-slice_fusion.14
  344.1 2.9 constant_dynamic-update-slice_fusion.13
  346.9 2.9 constant_dynamic-update-slice_fusion.12
  360.6 11.1 %multiply_convert_fusion = bf16[512,3584]{1,0:T(8,128)(2,1)S(1)} fusion(bf16[4096,3584]{1,0:T(8,128)(2,1)} %constant_dynamic-update-slice_fusion.23, s32[]{:T(128)S(6)} %select_n.53, f32[512]{0:T(512)S(1)} %add_rsqrt_fusion, bf16[512,2048]{1,0:T(8,128)(2,1)S(1)} %copy-done.16, f32[2048]{0:T(1024)S(1)} %copy-done.23), kind=kOutput, calls=%fused_computation.6 | convolution fusion | flops 7523008512 | bytes 20457476 | tf_op jit(solution)/shard_map/dot_general | solution.py:91
  374.6 2.8 convolution_convert_fusion.1
  381.8 1.6 fusion.13
  384.7 3.7 convert_multiply_fusion.5
  388.4 2.1 slice.415
  390.6 2.1 slice.353
  392.6 3.7 slice.350
  396.4 3.7 slice.351
  400.0 2.1 slice.352
  402.1 3.7 slice.355
  405.7 2.7 multiply_add_fusion.1
  408.5 2.5 slice.359
  411.0 2.5 slice.358
  413.4 2.5 slice.357
  415.9 2.5 slice.361
  418.4 2.0 multiply_add_fusion.2
  420.4 1.6 slice.411
  422.1 1.6 slice.365
  425.1 1.6 slice.364
  427.4 1.8 multiply_add_fusion.3
  433.6 1.6 multiply_add_fusion.4
  482.4 2.5 slice.413
  484.9 2.5 slice.356
  504.8 2.2 pad.138
  509.2 1.8 fusion.56
  511.7 2.4 pad.123
  514.1 1.7 add.340
  515.8 2.6 pad.125
  518.4 2.4 pad.141
  523.1 1.8 add.351
  524.9 2.1 fusion.55
  527.1 1.8 pad.124
  528.9 2.6 pad.143
  532.5 1.7 pad.142
  534.2 3.0 fusion.43
  537.9 2.1 add.352
  541.3 2.9 pad.144
  544.2 4.7 pad.145
  550.0 2.8 pad.126
  552.7 2.7 pad.127
  556.2 26.1 %all-gather = f32[8,1,512]{2,1,0:T(1,128)S(1)} all-gather(f32[1,1,512]{2,1,0:T(1,128)S(1)} %add_bitcast_fusion.1), channel_id=1, replica_groups=mesh['sp'=8,'tp'=4] {'sp'}, dimensions={0}, use_global_device_ids=true | all-gather | bytes 18432 | tf_op jit(solution)/shard_map/all_gather | solution.py:18
  583.1 26.1 %all-gather.1 = f32[8,1,512]{2,1,0:T(1,128)S(1)} all-gather(f32[1,1,512]{2,1,0:T(1,128)S(1)} %add_bitcast_fusion), channel_id=1, replica_groups=mesh['sp'=8,'tp'=4] {'sp'}, dimensions={0}, use_global_device_ids=true | all-gather | bytes 18432 | tf_op jit(solution)/shard_map/all_gather | solution.py:18
  610.3 6.0 convolution_convert_fusion
  616.4 27.6 %reduce-scatter.5.cloned.1.call-done = bf16[512,512]{1,0:T(8,128)(2,1)} async-done(((bf16[512,2048]{1,0:T(8,128)(2,1)}), bf16[512,512]{1,0:T(8,128)(2,1)}) %reduce-scatter.5.cloned.1.call-update) | async-done | bytes 524304 | tf_op jit(solution)/shard_map/reduce_scatter | solution.py:153
  644.0 2.9 add_convert_fusion
  (231 shorter events, 122.3 us)
Async XLA Ops:
  6.5 368.1 %copy-start = (bf16[512,2048]{1,0:T(8,128)(2,1)S(1)}, bf16[512,2048]{1,0:T(8,128)(2,1)}, u32[]{:S(2)}) copy-start(bf16[512,2048]{1,0:T(8,128)(2,1)} %param.38) | copy-start | bytes 6291460
  6.5 329.4 %copy-start.9 = (bf16[256,512]{1,0:T(8,128)(2,1)S(1)}, bf16[256,512]{1,0:T(8,128)(2,1)}, u32[]{:S(2)}) copy-start(bf16[256,512]{1,0:T(8,128)(2,1)} %param.23) | copy-start | bytes 786436
  6.5 330.2 %copy-start.10 = (bf16[256,512]{1,0:T(8,128)(2,1)S(1)}, bf16[256,512]{1,0:T(8,128)(2,1)}, u32[]{:S(2)}) copy-start(bf16[256,512]{1,0:T(8,128)(2,1)} %param.24) | copy-start | bytes 786436
  6.5 330.9 %copy-start.11 = (bf16[256,512]{1,0:T(8,128)(2,1)S(1)}, bf16[256,512]{1,0:T(8,128)(2,1)}, u32[]{:S(2)}) copy-start(bf16[256,512]{1,0:T(8,128)(2,1)} %param.25) | copy-start | bytes 786436
  6.5 331.7 %copy-start.12 = (bf16[256,512]{1,0:T(8,128)(2,1)S(1)}, bf16[256,512]{1,0:T(8,128)(2,1)}, u32[]{:S(2)}) copy-start(bf16[256,512]{1,0:T(8,128)(2,1)} %param.26) | copy-start | bytes 786436
  6.6 332.4 %copy-start.13 = (bf16[256,512]{1,0:T(8,128)(2,1)S(1)}, bf16[256,512]{1,0:T(8,128)(2,1)}, u32[]{:S(2)}) copy-start(bf16[256,512]{1,0:T(8,128)(2,1)} %param.27) | copy-start | bytes 786436
  6.6 271.7 %all-gather.4.cloned.1.call-start = ((), (), s32[]{:S(2)}) async-start(), calls=%async_computation.2 | async-start | bytes 2621440 | tf_op jit(solution)/shard_map/all_gather | solution.py:88
  13.6 46.1 %collective-permute-start = (bf16[256,3584]{1,0:T(8,128)(2,1)S(1)}, bf16[256,3584]{1,0:T(8,128)(2,1)S(1)}, u32[]{:S(2)}, u32[]{:S(2)}) collective-permute-start(bf16[256,3584]{1,0:T(8,128)(2,1)S(1)} %constant_dynamic-update-slice_fusion), channel_id=1, source_target_pairs={{0,4},{4,8},{8,12},{12,16},{16,20},{20,24},{24,28},{28,0},{1,5},{5... | collective-permute-start | bytes 5505032 | tf_op jit(solution)/shard_map/ppermute | solution.py:84
  59.6 1.3 copy-start.1
  60.9 43.9 %collective-permute-start.1 = (bf16[256,3584]{1,0:T(8,128)(2,1)S(1)}, bf16[256,3584]{1,0:T(8,128)(2,1)S(1)}, u32[]{:S(2)}, u32[]{:S(2)}) collective-permute-start(bf16[256,3584]{1,0:T(8,128)(2,1)S(1)} %collective-permute-done), channel_id=1, source_target_pairs={{0,4},{4,8},{8,12},{12,16},{16,20},{20,24},{24,28},{28,0},{1,5},{5... | collective-permute-start | bytes 5505032 | tf_op jit(solution)/shard_map/ppermute | solution.py:84
  104.8 1.2 copy-start.3
  106.0 43.0 %collective-permute-start.2 = (bf16[256,3584]{1,0:T(8,128)(2,1)S(1)}, bf16[256,3584]{1,0:T(8,128)(2,1)S(1)}, u32[]{:S(2)}, u32[]{:S(2)}) collective-permute-start(bf16[256,3584]{1,0:T(8,128)(2,1)S(1)} %collective-permute-done.1), channel_id=1, source_target_pairs={{0,4},{4,8},{8,12},{12,16},{16,20},{20,24},{24,28},{28,0},{1,5},{5... | collective-permute-start | bytes 5505032 | tf_op jit(solution)/shard_map/ppermute | solution.py:84
  149.0 1.3 copy-start.5
  150.3 42.2 %collective-permute-start.3 = (bf16[256,3584]{1,0:T(8,128)(2,1)S(1)}, bf16[256,3584]{1,0:T(8,128)(2,1)S(1)}, u32[]{:S(2)}, u32[]{:S(2)}) collective-permute-start(bf16[256,3584]{1,0:T(8,128)(2,1)S(1)} %collective-permute-done.2), channel_id=1, source_target_pairs={{0,4},{4,8},{8,12},{12,16},{16,20},{20,24},{24,28},{28,0},{1,5},{5... | collective-permute-start | bytes 5505032 | tf_op jit(solution)/shard_map/ppermute | solution.py:84
  192.5 1.2 copy-start.7
  193.7 41.4 %collective-permute-start.4 = (bf16[256,3584]{1,0:T(8,128)(2,1)S(1)}, bf16[256,3584]{1,0:T(8,128)(2,1)}, u32[]{:S(2)}, u32[]{:S(2)}) collective-permute-start(bf16[256,3584]{1,0:T(8,128)(2,1)S(1)} %collective-permute-done.3), channel_id=1, source_target_pairs={{0,4},{4,8},{8,12},{12,16},{16,20},{20,24},{24,28},{28,0},{1,5},{5... | collective-permute-start | bytes 5505032 | tf_op jit(solution)/shard_map/ppermute | solution.py:84
  235.1 40.8 %collective-permute-start.5 = (bf16[256,3584]{1,0:T(8,128)(2,1)}, bf16[256,3584]{1,0:T(8,128)(2,1)}, u32[]{:S(2)}, u32[]{:S(2)}) collective-permute-start(bf16[256,3584]{1,0:T(8,128)(2,1)} %collective-permute-done.4), channel_id=1, source_target_pairs={{0,4},{4,8},{8,12},{12,16},{16,20},{20,24},{24,28},{28,0},{1,5},{5... | collective-permute-start | bytes 5505032 | tf_op jit(solution)/shard_map/ppermute | solution.py:84
  235.1 381.2 %reduce-scatter.3.cloned.1.call-start = ((), (), s32[]{:S(2)}) async-start(), calls=%async_computation.3 | async-start | bytes 2621440 | tf_op jit(solution)/shard_map/reduce_scatter | solution.py:150
  275.9 39.9 %collective-permute-start.6 = (bf16[256,3584]{1,0:T(8,128)(2,1)}, bf16[256,3584]{1,0:T(8,128)(2,1)}, u32[]{:S(2)}, u32[]{:S(2)}) collective-permute-start(bf16[256,3584]{1,0:T(8,128)(2,1)} %collective-permute-done.5), channel_id=1, source_target_pairs={{0,4},{4,8},{8,12},{12,16},{16,20},{20,24},{24,28},{28,0},{1,5},{5... | collective-permute-start | bytes 5505032 | tf_op jit(solution)/shard_map/ppermute | solution.py:84
  278.3 61.4 %copy-start.14 = (bf16[256,512]{1,0:T(8,128)(2,1)S(1)}, bf16[256,512]{1,0:T(8,128)(2,1)}, u32[]{:S(2)}) copy-start(bf16[256,512]{1,0:T(8,128)(2,1)} %param.28) | copy-start | bytes 786436
  278.3 62.2 %copy-start.15 = (bf16[256,512]{1,0:T(8,128)(2,1)S(1)}, bf16[256,512]{1,0:T(8,128)(2,1)}, u32[]{:S(2)}) copy-start(bf16[256,512]{1,0:T(8,128)(2,1)} %param.29) | copy-start | bytes 786436
  278.3 71.5 %copy-start.8 = (bf16[256,3584]{1,0:T(8,128)(2,1)S(1)}, bf16[256,3584]{1,0:T(8,128)(2,1)}, u32[]{:S(2)}) copy-start(bf16[256,3584]{1,0:T(8,128)(2,1)} %copy-done.7) | copy-start | bytes 5505028
  278.3 72.9 %copy-start.6 = (bf16[256,3584]{1,0:T(8,128)(2,1)S(1)}, bf16[256,3584]{1,0:T(8,128)(2,1)}, u32[]{:S(2)}) copy-start(bf16[256,3584]{1,0:T(8,128)(2,1)} %copy-done.5) | copy-start | bytes 5505028
  278.3 74.2 %copy-start.4 = (bf16[256,3584]{1,0:T(8,128)(2,1)S(1)}, bf16[256,3584]{1,0:T(8,128)(2,1)}, u32[]{:S(2)}) copy-start(bf16[256,3584]{1,0:T(8,128)(2,1)} %copy-done.3) | copy-start | bytes 5505028
  278.3 75.7 %copy-start.2 = (bf16[256,3584]{1,0:T(8,128)(2,1)S(1)}, bf16[256,3584]{1,0:T(8,128)(2,1)}, u32[]{:S(2)}) copy-start(bf16[256,3584]{1,0:T(8,128)(2,1)} %copy-done.1) | copy-start | bytes 5505028
  280.6 80.0 %copy-start.16 = (bf16[512,2048]{1,0:T(8,128)(2,1)S(1)}, bf16[512,2048]{1,0:T(8,128)(2,1)}, u32[]{:S(2)}) copy-start(bf16[512,2048]{1,0:T(8,128)(2,1)} %all-gather.4.cloned.1.call-done) | copy-start | bytes 6291460
  280.6 80.0 %copy-start.23 = (f32[2048]{0:T(1024)S(1)}, f32[2048]{0:T(1024)}, u32[]{:S(2)}) copy-start(f32[2048]{0:T(1024)} %param.22) | copy-start | bytes 24580
  371.7 2.9 copy-start.18
  371.7 13.0 %copy-start.21 = (f32[512]{0:T(512)S(1)}, f32[512]{0:T(512)}, u32[]{:S(2)}) copy-start(f32[512]{0:T(512)} %param.36) | copy-start | bytes 6148
  371.7 13.0 %copy-start.22 = (f32[512]{0:T(512)S(1)}, f32[512]{0:T(512)}, u32[]{:S(2)}) copy-start(f32[512]{0:T(512)} %param.35) | copy-start | bytes 6148
  371.9 2.7 collective-permute-start.7
  373.3 4.4 collective-permute-start.8
  377.4 266.6 %reduce-scatter.5.cloned.1.call-start = ((), (), s32[]{:S(2)}) async-start(), calls=%async_computation.4 | async-start | bytes 2621440 | tf_op jit(solution)/shard_map/reduce_scatter | solution.py:153
  378.2 0.8 copy-start.17
  471.8 137.3 %copy-start.19 = (f32[512]{0:T(512)S(1)}, f32[512]{0:T(512)}, u32[]{:S(2)}) copy-start(f32[512]{0:T(512)} %custom-call) | copy-start | bytes 6148
  471.8 137.3 %copy-start.20 = (f32[512]{0:T(512)S(1)}, f32[512]{0:T(512)}, u32[]{:S(2)}) copy-start(f32[512]{0:T(512)} %custom-call.1) | copy-start | bytes 6148
Sparse Core Ops, SparseCore 0:
  235.3 23.2 all-gather.3
  377.6 29.7 reduce-scatter.2
  616.5 27.4 reduce-scatter.4
